TPU v7x, 32 devices: a whole 2x2x4 slice. The times are simulated.
32 devices in a mesh: ep: 16 (over z, y, x), tp: 2 (over core).
Axes of the slice: x: 2, y: 2, z: 4, core: 2. Of those that a mesh axis runs over, the one named last changes fastest.
Arguments:
- residual_in: bfloat16 [256, 1024], P('ep'), may hold values from -6 to 6
- lengths: int32 [256], P('ep'), may hold values from 64 to 1024
- cache_keys: bfloat16 [256, 2, 1024, 128], P('ep', 'tp'), may hold values from -7 to 7
- cache_values: bfloat16 [256, 2, 1024, 128], P('ep', 'tp'), may hold values from -6 to 6
- attend_gain: bfloat16 [1024], replicated, may hold values from 0.099609375 to 1.8984375
- query_proj: bfloat16 [1024, 512], P(None, 'tp'), may hold values from -0.1875 to 0.1875
- key_proj: bfloat16 [1024, 256], P(None, 'tp'), may hold values from -0.1875 to 0.1875
- value_proj: bfloat16 [1024, 256], P(None, 'tp'), may hold values from -0.1875 to 0.1875
- lambdas: float32 [4], P('tp'), may hold values from 0.3 to 0.8
- head_gain: bfloat16 [128], replicated, may hold values from 0.099609375 to 1.8984375
- out_proj: bfloat16 [512, 1024], P('tp'), may hold values from -0.25 to 0.25
- channel_gain: bfloat16 [1024], replicated, may hold values from 0.099609375 to 1.8984375
- routes: int32 [256, 6], P('ep'), may hold values from 0 to 15, all different within a row; in each aligned block of 16 rows (0 to 15, 16 to 31, ...) at most 12 rows name the same one
- route_weight: float32 [256, 6], P('ep'), may hold values from 0.1 to 1
- expert_gate: bfloat16 [16, 1024, 512], P('ep', None, 'tp'), may hold values from -0.1875 to 0.1875
- expert_up: bfloat16 [16, 1024, 512], P('ep', None, 'tp'), may hold values from -0.1875 to 0.1875
- expert_down: bfloat16 [16, 512, 1024], P('ep', 'tp'), may hold values from -0.25 to 0.25
- dense_gate: bfloat16 [1024, 4096], P(None, ('ep', 'tp')), may hold values from -0.1875 to 0.1875
- dense_up: bfloat16 [1024, 4096], P(None, ('ep', 'tp')), may hold values from -0.1875 to 0.1875
- dense_down: bfloat16 [4096, 1024], P(('ep', 'tp')), may hold values from -0.09375 to 0.09375
- dense_mixer: bfloat16 [1024], replicated, may hold values from -0.1875 to 0.1875
Outputs:
- residual_out: bfloat16 [256, 1024], P('ep')
- new_keys: bfloat16 [256, 2, 128], P('ep', 'tp')
- new_values: bfloat16 [256, 2, 128], P('ep', 'tp')
Inputs may be any that keep to these rules, and one draw needn't show every extreme that they name: `routes`: each row names 6 different experts; in each aligned block of 16 rows (the rows of one index of ep) no expert is named by more than 12 rows, and in some blocks one expert is named by exactly 12 rows.
All inputs are finite; a program needn't handle non-finite values.
Results may differ from a plain program's by a relative error of at most 0.015.
Values may be sent and summed in bfloat16 or wider, within the bound.
A program may use at most 64 MiB of HBM per device.

v0:
```python
import functools

import jax
import jax.numpy as jnp
import numpy as np
from jax import lax
from jax.experimental import pallas as pl
from jax.experimental.pallas import tpu as pltpu
from jax.sharding import PartitionSpec as P

HEAD = 64
NORM_EPSILON = 1e-06
ROTARY_BASE = 10000.0
HEAD_SCALE = 0.8
KEY_CHUNKS = 4
MESH = pl.DeviceIdType.MESH
F32 = jnp.float32
BF16 = jnp.bfloat16


def norm_scale(vectors, gain_vector):
    mean_square = jnp.mean(vectors * vectors, axis=-1, keepdims=True)
    return vectors * lax.rsqrt(mean_square + NORM_EPSILON) * gain_vector


def mm(a, b):
    return jnp.dot(a, b, preferred_element_type=F32)


def row_of(ref):
    return ref[...].astype(F32).reshape(1, ref.shape[0])


def silu(v):
    return v / (1.0 + jnp.exp(-v))


def kernel(
    n,
    len_ref,
    lam_ref,
    inv_ref,
    res_ref,
    again_ref,
    hgain_ref,
    cgain_ref,
    mixer_ref,
    routes_ref,
    rw_ref,
    ck_hbm,
    cv_hbm,
    wq_hbm,
    wk_hbm,
    wv_hbm,
    wo_hbm,
    eg_hbm,
    eu_hbm,
    ed_hbm,
    dg_hbm,
    du_hbm,
    dd_hbm,
    out_ref,
    nk_ref,
    nv_ref,
    ck,
    cv,
    wq,
    wk,
    wv,
    wo,
    eg,
    eu,
    ed,
    dg,
    du,
    dd,
    pos,
    qs,
    es,
    den,
    att,
    part,
    part_in,
    mid,
    nrm,
    tabf,
    tab,
    xs,
    ys,
    rs,
    ob,
    small_sem,
    key_sem,
    val_sem,
    own_sem,
    wsend,
    wrecv,
    tsend,
    trecv,
    xsend,
    xrecv,
    ysend,
    yrecv,
    psem,
    osem,
):
    seqs, width = res_ref.shape
    half = xs.shape[1]
    me = lax.axis_index("ep")
    tp = lax.axis_index("tp")
    other = 1 - tp
    chunk = seqs // KEY_CHUNKS

    bar = pltpu.get_barrier_semaphore()
    pl.semaphore_signal(bar, inc=1, device_id=(me, other), device_id_type=MESH)

    def greet(k, c):
        pl.semaphore_signal(
            bar, inc=1, device_id=(lax.rem(me + k, n), tp), device_id_type=MESH
        )
        return c

    lax.fori_loop(1, n, greet, 0)

    small = [
        pltpu.make_async_copy(a, b, small_sem.at[i])
        for i, (a, b) in enumerate(((wq_hbm, wq), (wk_hbm, wk), (wv_hbm, wv), (wo_hbm, wo)))
    ]
    keys = [
        pltpu.make_async_copy(
            ck_hbm.at[pl.ds(i * chunk, chunk)], ck.at[pl.ds(i * chunk, chunk)], key_sem.at[i]
        )
        for i in range(KEY_CHUNKS)
    ]
    vals = [
        pltpu.make_async_copy(
            cv_hbm.at[pl.ds(i * chunk, chunk)], cv.at[pl.ds(i * chunk, chunk)], val_sem.at[i]
        )
        for i in range(KEY_CHUNKS)
    ]
    weight_pairs = (
        (eg_hbm, eg),
        (eu_hbm, eu),
        (ed_hbm, ed),
        (dg_hbm, dg),
        (du_hbm, du),
        (dd_hbm, dd),
    )
    own = [
        pltpu.make_async_copy(a, b.at[0], own_sem.at[i]) for i, (a, b) in enumerate(weight_pairs)
    ]
    for c in small[:3] + keys + vals + small[3:] + own:
        c.start()

    lanes = tabf.shape[1]
    expert_row = lax.broadcasted_iota(jnp.int32, (lanes, seqs), 0)
    routes = routes_ref[...]
    rweights = rw_ref[...]
    table = jnp.zeros((lanes, seqs), F32)
    for k in range(routes.shape[0]):
        table = table + jnp.where(expert_row == routes[k : k + 1], rweights[k : k + 1], 0.0)
    tabf[...] = table.T
    tab[me] = tabf[pl.ds(pl.multiple_of(tp * half, half), half), :]

    for s in range(seqs):
        pos[s : s + 1, :] = jnp.full((1, 2 * HEAD), len_ref[s].astype(F32), F32)
    angles = pos[...] * inv_ref[...]
    cosine = jnp.cos(angles)
    lane = lax.broadcasted_iota(jnp.int32, (seqs, 2 * HEAD), 1)
    front = (lane % HEAD) < HEAD // 2
    sine = jnp.where(front, -1.0, 1.0) * jnp.sin(angles)

    def rotate(u):
        swapped = jnp.where(
            front,
            pltpu.roll(u, 2 * HEAD - HEAD // 2, 1),
            pltpu.roll(u, HEAD // 2, 1),
        )
        return (u * cosine + swapped * sine).astype(BF16)

    residual = res_ref[...].astype(F32)
    normed = norm_scale(residual, row_of(again_ref)).astype(BF16)
    for c in small[:3]:
        c.wait()
    queries = mm(normed, wq[...])
    new_keys = rotate(mm(normed, wk[...]))
    new_values = mm(normed, wv[...]).astype(BF16)
    nk_ref[...] = new_keys
    nv_ref[...] = new_values
    groups = queries.shape[1] // (2 * HEAD)
    rows = qs.shape[1]
    qs[...] = jnp.zeros_like(qs)
    for g in range(groups):
        turned = rotate(queries[:, g * 2 * HEAD : (g + 1) * 2 * HEAD]).astype(F32) * (
            HEAD**-0.5
        )
        for m in range(2):
            qs[:, 2 * g + m, :] = jnp.where(lane // HEAD == m, turned, 0.0)

    pl.semaphore_wait(bar, n)
    swaps = [
        pltpu.make_async_remote_copy(
            src_ref=a,
            dst_ref=b.at[1],
            send_sem=wsend.at[i],
            recv_sem=wrecv.at[i],
            device_id=(me, other),
            device_id_type=MESH,
        )
        for i, (a, b) in enumerate(weight_pairs)
    ]
    for c in swaps:
        c.start()

    def to_peer(src, dst, ssem, rsem, k):
        return pltpu.make_async_remote_copy(
            src_ref=src,
            dst_ref=dst,
            send_sem=ssem.at[k],
            recv_sem=rsem.at[k],
            device_id=(lax.rem(me + k, n), tp),
            device_id_type=MESH,
        )

    def send_table(k, c):
        to_peer(tab.at[me], tab.at[me], tsend, trecv, k).start()
        return c

    lax.fori_loop(1, n, send_table, 0)

    position = lax.broadcasted_iota(jnp.int32, (rows, ck.shape[1]), 1)
    for s in range(seqs):
        if s % chunk == 0:
            keys[s // chunk].wait()
        scores = lax.dot_general(
            qs[s].astype(BF16), ck[s], (((1,), (1,)), ((), ())), preferred_element_type=F32
        )
        exponent = jnp.where(position < len_ref[s], jnp.exp(scores), 0.0)
        den[s] = jnp.broadcast_to(jnp.sum(exponent, axis=-1, keepdims=True), den.shape[1:])
        es[s] = exponent.astype(BF16)
    for s in range(seqs):
        if s % chunk == 0:
            vals[s // chunk].wait()
        att[s] = mm(es[s], cv[s])
    kf = new_keys.astype(F32).reshape(seqs, 1, 2 * HEAD)
    vf = new_values.astype(F32).reshape(seqs, 1, new_values.shape[1])
    own_exp = jnp.exp(jnp.sum(qs[...] * kf, axis=-1, keepdims=True))
    att[...] = (att[...] + own_exp * vf) / (den[...] + own_exp)
    small[3].wait()
    head_gain = row_of(hgain_ref)
    heads = [
        (
            norm_scale(att[:, 2 * g, :] - lam_ref[g] * att[:, 2 * g + 1, :], head_gain)
            * HEAD_SCALE
        ).astype(BF16)
        for g in range(groups)
    ]
    partial = mm(jnp.concatenate(heads, axis=1), wo[...]).astype(BF16)
    part[...] = partial
    swap = pltpu.make_async_remote_copy(
        src_ref=part,
        dst_ref=part_in,
        send_sem=psem.at[0],
        recv_sem=psem.at[1],
        device_id=(me, other),
        device_id_type=MESH,
    )
    swap.start()
    swap.wait()
    middle = (residual + (partial.astype(F32) + part_in[...].astype(F32))).astype(BF16)
    middle = middle.astype(F32)
    mid[...] = middle
    nrm[...] = norm_scale(middle, row_of(cgain_ref))
    mine = pl.ds(pl.multiple_of(tp * half, half), half)
    xs[me] = nrm[mine, :].astype(BF16)

    def send_rows(k, c):
        to_peer(xs.at[me], xs.at[me], xsend, xrecv, k).start()
        return c

    lax.fori_loop(1, n, send_rows, 0)

    for c in own:
        c.wait()
    for c in swaps:
        c.wait()

    def take_rows(k, c):
        src = lax.rem(me + n - k, n)
        to_peer(tab.at[me], tab.at[src], tsend, trecv, k).wait()
        to_peer(xs.at[me], xs.at[src], xsend, xrecv, k).wait()
        return c

    lax.fori_loop(1, n, take_rows, 0)

    count = n * half
    xf = xs[...].astype(F32).reshape(count, width)
    x = xf.astype(BF16)
    switch = 1.0 / (
        1.0 + jnp.exp(-jnp.sum(xf * row_of(mixer_ref), axis=-1, keepdims=True))
    )
    table_all = tab[...].reshape(count, lanes)
    weight = jnp.sum(
        jnp.where(lax.broadcasted_iota(jnp.int32, (count, lanes), 1) == me, table_all, 0.0),
        axis=-1,
        keepdims=True,
    )
    total = None
    for gate, up, down, scale in ((eg, eu, ed, weight), (dg, du, dd, switch)):
        units = gate.shape[2]
        merge = units % 128 == 0
        for slots in ((0, 1),) if merge else ((0,), (1,)):
            gw = jnp.concatenate([gate[i] for i in slots], axis=1) if merge else gate[slots[0]]
            uw = jnp.concatenate([up[i] for i in slots], axis=1) if merge else up[slots[0]]
            dw = jnp.concatenate([down[i] for i in slots], axis=0) if merge else down[slots[0]]
            hidden = (silu(mm(x, gw)) * mm(x, uw) * scale).astype(BF16)
            term = mm(hidden, dw)
            total = term if total is None else total + term
    ys[...] = total.reshape(n, half, width).astype(BF16)
    rs[me] = ys[me]

    def send_sums(k, c):
        peer = lax.rem(me + k, n)
        to_peer(ys.at[peer], rs.at[me], ysend, yrecv, k).start()
        return c

    lax.fori_loop(1, n, send_sums, 0)

    def take_sums(k, c):
        src = lax.rem(me + n - k, n)
        to_peer(ys.at[src], rs.at[src], ysend, yrecv, k).wait()
        return c

    lax.fori_loop(1, n, take_sums, 0)
    ob[tp] = (mid[mine, :] + jnp.sum(rs[...].astype(F32), axis=0)).astype(BF16)
    last = pltpu.make_async_remote_copy(
        src_ref=ob.at[tp],
        dst_ref=ob.at[tp],
        send_sem=osem.at[0],
        recv_sem=osem.at[1],
        device_id=(me, other),
        device_id_type=MESH,
    )
    last.start()
    last.wait()
    out_ref[...] = ob[...].astype(F32).reshape(seqs, width).astype(BF16)


def hand_over(*refs):
    count = len(refs) // 2
    for source, target in zip(refs[:count], refs[count:]):
        target[...] = source[...]


def per_device(
    n,
    residual_in,
    lengths,
    cache_keys,
    cache_values,
    attend_gain,
    query_proj,
    key_proj,
    value_proj,
    lambdas,
    head_gain,
    out_proj,
    channel_gain,
    routes,
    route_weight,
    expert_gate,
    expert_up,
    expert_down,
    dense_gate,
    dense_up,
    dense_down,
    dense_mixer,
):
    seqs, width = residual_in.shape
    _, kv_local, length, key_width = cache_keys.shape
    value_width = cache_values.shape[3]
    half = seqs // 2
    lanes = -(-n // 128) * 128
    rows = 8
    inverse = ROTARY_BASE ** (-np.arange(HEAD // 2, dtype=np.float32) / (HEAD // 2))
    inverse = jnp.asarray(np.tile(inverse.astype(np.float32), 4)[None, :])
    vmem = pl.BlockSpec(memory_space=pltpu.VMEM)
    smem = pl.BlockSpec(memory_space=pltpu.SMEM)
    anym = pl.BlockSpec(memory_space=pl.ANY)

    def two(w):
        return pltpu.VMEM((2,) + w.shape, BF16)

    eg, eu, ed = expert_gate[0], expert_up[0], expert_down[0]
    big = (
        cache_keys.reshape(seqs, length, key_width),
        cache_values.reshape(seqs, length, value_width),
        query_proj,
        key_proj,
        value_proj,
        out_proj,
        eg,
        eu,
        ed,
        dense_gate,
        dense_up,
        dense_down,
    )
    dma = pltpu.SemaphoreType.DMA
    out, nk, nv = pl.pallas_call(
        functools.partial(kernel, n),
        out_shape=(
            jax.ShapeDtypeStruct((seqs, width), BF16),
            jax.ShapeDtypeStruct((seqs, key_width), BF16),
            jax.ShapeDtypeStruct((seqs, value_width), BF16),
        ),
        in_specs=[smem, smem] + [vmem] * 8 + [anym] * len(big),
        out_specs=(vmem, vmem, vmem),
        scratch_shapes=[pltpu.VMEM(w.shape, BF16) for w in big[:6]]
        + [two(w) for w in big[6:]]
        + [
            pltpu.VMEM((seqs, 2 * HEAD), F32),
            pltpu.VMEM((seqs, rows, key_width), F32),
            pltpu.VMEM((seqs, rows, length), BF16),
            pltpu.VMEM((seqs, rows, value_width), F32),
            pltpu.VMEM((seqs, rows, value_width), F32),
            pltpu.VMEM((seqs, width), BF16),
            pltpu.VMEM((seqs, width), BF16),
            pltpu.VMEM((seqs, width), F32),
            pltpu.VMEM((seqs, width), F32),
            pltpu.VMEM((seqs, lanes), F32),
            pltpu.VMEM((n, half, lanes), F32),
            pltpu.VMEM((n, half, width), BF16),
            pltpu.VMEM((n, half, width), BF16),
            pltpu.VMEM((n, half, width), BF16),
            pltpu.VMEM((2, half, width), BF16),
            dma((4,)),
            dma((KEY_CHUNKS,)),
            dma((KEY_CHUNKS,)),
            dma((6,)),
            dma((6,)),
            dma((6,)),
            dma((n,)),
            dma((n,)),
            dma((n,)),
            dma((n,)),
            dma((n,)),
            dma((n,)),
            dma((2,)),
            dma((2,)),
        ],
        compiler_params=pltpu.CompilerParams(
            collective_id=0, has_side_effects=True, vmem_limit_bytes=56 * 1024 * 1024
        ),
    )(
        lengths,
        lambdas,
        inverse,
        residual_in,
        attend_gain,
        head_gain,
        channel_gain,
        dense_mixer,
        routes.T,
        route_weight.T,
        *big,
    )
    out, nk, nv = pl.pallas_call(
        hand_over,
        out_shape=tuple(jax.ShapeDtypeStruct(a.shape, BF16) for a in (out, nk, nv)),
        in_specs=[vmem] * 3,
        out_specs=(vmem, vmem, vmem),
    )(out, nk, nv)
    return (
        out,
        nk.reshape(seqs, kv_local, key_width),
        nv.reshape(seqs, kv_local, value_width),
    )


def solution(mesh):
    return jax.shard_map(
        functools.partial(per_device, mesh.shape["ep"]),
        mesh=mesh,
        in_specs=(
            P("ep", None),
            P("ep"),
            P("ep", "tp", None, None),
            P("ep", "tp", None, None),
            P(),
            P(None, "tp"),
            P(None, "tp"),
            P(None, "tp"),
            P("tp"),
            P(),
            P("tp", None),
            P(),
            P("ep", None),
            P("ep", None),
            P("ep", None, "tp"),
            P("ep", None, "tp"),
            P("ep", "tp", None),
            P(None, ("ep", "tp")),
            P(None, ("ep", "tp")),
            P(("ep", "tp"), None),
            P(),
        ),
        out_specs=(P("ep", None), P("ep", "tp", None), P("ep", "tp", None)),
        check_vma=False,
    )
```

profile of v0, /device:TPU:0, one launch (start us, length us, event | category | flops | bytes accessed | tf_op | source)
XLA Modules:
  0.0 31.7 jit_solution(2605467654452301290)
XLA Ops:
  0.6 29.6 %shard_map.229 = (bf16[16,1024]{1,0:T(8,128)(2,1)}, bf16[16,128]{1,0:T(8,128)(2,1)}, bf16[16,128]{1,0:T(8,128)(2,1)}) custom-call(s32[16]{0:T(128)} %len_ref.1, f32[2]{0:T(128)} %lam_ref.1, f32[1,128]{1,0:T(1,128)} %constant.2.clone.inv_ref, bf16[16,1024]{1,0:T(8,128)(2,1)} %res_ref.1, bf16[1024]{0:T(1024)(128)(2,1)} %again_ref.1, bf16[128]{0:T(256)(128)(2,1)} %hgain_ref.1, ...), custom_call_target="tpu_custom_call" | custom-call | tf_op jit(solution)/shard_map/pallas_call | solution.py:410
  30.3 1.4 %shard_map.230 = (bf16[16,1024]{1,0:T(8,128)(2,1)}, bf16[16,128]{1,0:T(8,128)(2,1)}, bf16[16,128]{1,0:T(8,128)(2,1)}) custom-call(bf16[16,1024]{1,0:T(8,128)(2,1)} %get-tuple-element.9.refs_0_, bf16[16,128]{1,0:T(8,128)(2,1)} %get-tuple-element.10.refs_1_, bf16[16,128]{1,0:T(8,128)(2,1)} %get-tuple-element.11.refs_2_), custom_call_target="tpu_custom_call" | custom-call | tf_op jit(solution)/shard_map/pallas_call | solution.py:468
where the time goes:
time: 31.9 us; the launch traced here: 31.7 us
  Pallas kernels  31 us (97%)
  between operations  0.65 us (2%)
    pallas_call x1, Pallas kernels, per_device(): pl.pallas_call(functools.partial(kernel, n), out_shape=(jax.ShapeDtypeStr...  29.6 us
    pallas_call x1, Pallas kernels, per_device(): pl.pallas_call(hand_over, out_shape=tuple((jax.ShapeDtypeStruct(a.shape,...  1.39 us

commit v1 on v0

v1 whole, which is shorter than its diff:
```python
import functools

import jax
import jax.numpy as jnp
import numpy as np
from jax import lax
from jax.experimental import pallas as pl
from jax.experimental.pallas import tpu as pltpu
from jax.sharding import PartitionSpec as P

HEAD = 64
NORM_EPSILON = 1e-06
ROTARY_BASE = 10000.0
HEAD_SCALE = 0.8
KEY_CHUNKS = 4
MESH = pl.DeviceIdType.MESH
F32 = jnp.float32
BF16 = jnp.bfloat16


def norm_scale(vectors, gain_vector):
    mean_square = jnp.mean(vectors * vectors, axis=-1, keepdims=True)
    return vectors * lax.rsqrt(mean_square + NORM_EPSILON) * gain_vector


def mm(a, b):
    return jnp.dot(a, b, preferred_element_type=F32)


def row_of(ref):
    return ref[...].astype(F32).reshape(1, ref.shape[0])


def silu(v):
    return v / (1.0 + jnp.exp(-v))


def kernel(
    n,
    len_hbm,
    lam_hbm,
    inv_hbm,
    res_hbm,
    again_hbm,
    hgain_hbm,
    cgain_hbm,
    mixer_hbm,
    routes_hbm,
    rw_hbm,
    ck_hbm,
    cv_hbm,
    wq_hbm,
    wk_hbm,
    wv_hbm,
    wo_hbm,
    eg_hbm,
    eu_hbm,
    ed_hbm,
    dg_hbm,
    du_hbm,
    dd_hbm,
    out_ref,
    nk_ref,
    nv_ref,
    lens,
    lam,
    inv,
    res,
    again,
    hgain,
    cgain,
    mixer,
    routes_v,
    rw_v,
    ck,
    cv,
    wq,
    wk,
    wv,
    wo,
    eg,
    eu,
    ed,
    dg,
    du,
    dd,
    pos,
    qs,
    es,
    den,
    att,
    part,
    part_in,
    mid,
    tabf,
    tab,
    xs,
    ys,
    rs,
    ob,
    small_sem,
    proj_sem,
    key_sem,
    val_sem,
    own_sem,
    wsend,
    wrecv,
    link,
):
    seqs, width = res.shape
    half = xs.shape[1]
    me = lax.axis_index("ep")
    tp = lax.axis_index("tp")
    other = 1 - tp
    chunk = seqs // KEY_CHUNKS

    small = [
        pltpu.make_async_copy(a, b, small_sem.at[i])
        for i, (a, b) in enumerate(
            (
                (len_hbm, lens),
                (inv_hbm, inv),
                (res_hbm, res),
                (again_hbm, again),
                (routes_hbm, routes_v),
                (rw_hbm, rw_v),
                (lam_hbm, lam),
                (hgain_hbm, hgain),
                (cgain_hbm, cgain),
                (mixer_hbm, mixer),
            )
        )
    ]
    proj = [
        pltpu.make_async_copy(a, b, proj_sem.at[i])
        for i, (a, b) in enumerate(((wq_hbm, wq), (wk_hbm, wk), (wv_hbm, wv), (wo_hbm, wo)))
    ]
    keys = [
        pltpu.make_async_copy(
            ck_hbm.at[pl.ds(i * chunk, chunk)], ck.at[pl.ds(i * chunk, chunk)], key_sem.at[i]
        )
        for i in range(KEY_CHUNKS)
    ]
    vals = [
        pltpu.make_async_copy(
            cv_hbm.at[pl.ds(i * chunk, chunk)], cv.at[pl.ds(i * chunk, chunk)], val_sem.at[i]
        )
        for i in range(KEY_CHUNKS)
    ]
    weight_pairs = (
        (eg_hbm, eg),
        (eu_hbm, eu),
        (ed_hbm, ed),
        (dg_hbm, dg),
        (du_hbm, du),
        (dd_hbm, dd),
    )
    own = [
        pltpu.make_async_copy(a, b.at[0], own_sem.at[i]) for i, (a, b) in enumerate(weight_pairs)
    ]
    for c in small[:4] + proj[:3] + keys[:1] + small[4:] + keys[1:2]:
        c.start()

    bar = pltpu.get_barrier_semaphore()
    pl.semaphore_signal(bar, inc=1, device_id=(me, other), device_id_type=MESH)

    def greet(k, c):
        pl.semaphore_signal(
            bar, inc=1, device_id=(lax.rem(me + k, n), tp), device_id_type=MESH
        )
        return c

    lax.fori_loop(1, n, greet, 0)

    small[0].wait()
    for s in range(seqs):
        pos[s : s + 1, :] = jnp.full((1, 2 * HEAD), lens[s].astype(F32), F32)
    small[1].wait()
    angles = pos[...] * inv[...]
    cosine = jnp.cos(angles)
    lane = lax.broadcasted_iota(jnp.int32, (seqs, 2 * HEAD), 1)
    front = (lane % HEAD) < HEAD // 2
    sine = jnp.where(front, -1.0, 1.0) * jnp.sin(angles)

    def rotate(u):
        swapped = jnp.where(
            front,
            pltpu.roll(u, 2 * HEAD - HEAD // 2, 1),
            pltpu.roll(u, HEAD // 2, 1),
        )
        return (u * cosine + swapped * sine).astype(BF16)

    small[2].wait()
    small[3].wait()
    residual = res[...].astype(F32)
    normed = norm_scale(residual, row_of(again)).astype(BF16)
    for c in proj[:3]:
        c.wait()
    for c in vals[:2] + proj[3:]:
        c.start()
    queries = mm(normed, wq[...])
    new_keys = rotate(mm(normed, wk[...]))
    new_values = mm(normed, wv[...]).astype(BF16)
    nk_ref[...] = new_keys
    nv_ref[...] = new_values
    groups = queries.shape[1] // (2 * HEAD)
    rows = qs.shape[1]
    qs[...] = jnp.zeros_like(qs)
    for g in range(groups):
        turned = rotate(queries[:, g * 2 * HEAD : (g + 1) * 2 * HEAD]).astype(F32) * (
            HEAD**-0.5
        )
        for m in range(2):
            qs[:, 2 * g + m, :] = jnp.where(lane // HEAD == m, turned, 0.0)

    for c in small[4:]:
        c.wait()
    lanes = tabf.shape[1]
    expert_row = lax.broadcasted_iota(jnp.int32, (lanes, seqs), 0)
    routes = routes_v[...]
    rweights = rw_v[...]
    table = jnp.zeros((lanes, seqs), F32)
    for k in range(routes.shape[0]):
        table = table + jnp.where(expert_row == routes[k : k + 1], rweights[k : k + 1], 0.0)
    tabf[...] = table.T
    mine = pl.ds(pl.multiple_of(tp * half, half), half)
    tab[me] = tabf[mine, :]

    def to_peer(src, dst, k, peer):
        return pltpu.make_async_remote_copy(
            src_ref=src,
            dst_ref=dst,
            send_sem=link.at[2 * k],
            recv_sem=link.at[2 * k + 1],
            device_id=peer,
            device_id_type=MESH,
        )

    def each_peer(send):
        if n & (n - 1) == 0 and n <= 16:
            bits = [lax.rem(lax.div(me, 1 << b), 2) for b in range(n.bit_length() - 1)]
            for k in range(n - 1, 0, -1):
                send(
                    sum(
                        (1 << b) * (1 - bit if k >> b & 1 else bit)
                        for b, bit in enumerate(bits)
                    )
                )
        else:

            def step(k, c):
                send(lax.rem(me + k, n))
                return c

            lax.fori_loop(1, n, step, 0)

    def all_but_one(buffer, k):
        block = buffer.at[pl.ds(0, n - 1)]
        return to_peer(block, block, k, (me, other))

    pl.semaphore_wait(bar, n)
    swaps = [
        pltpu.make_async_remote_copy(
            src_ref=a,
            dst_ref=b.at[1],
            send_sem=wsend.at[i],
            recv_sem=wrecv.at[i],
            device_id=(me, other),
            device_id_type=MESH,
        )
        for i, (a, b) in enumerate(weight_pairs)
    ]
    for i in (0, 1):
        own[i].start()
        swaps[i].start()
    each_peer(lambda peer: to_peer(tab.at[me], tab.at[me], 0, (peer, tp)).start())

    position = lax.broadcasted_iota(jnp.int32, (rows, ck.shape[1]), 1)
    kf = new_keys.astype(F32).reshape(seqs, 1, 2 * HEAD)
    vf = new_values.astype(F32).reshape(seqs, 1, new_values.shape[1])
    own_exp = jnp.exp(jnp.sum(qs[...] * kf, axis=-1, keepdims=True))
    head_gain = row_of(hgain)

    def score(g):
        for s in range(g * half, (g + 1) * half):
            if s % chunk == 0:
                keys[s // chunk].wait()
                if s // chunk + 2 < KEY_CHUNKS:
                    keys[s // chunk + 2].start()
            scores = lax.dot_general(
                qs[s].astype(BF16), ck[s], (((1,), (1,)), ((), ())), preferred_element_type=F32
            )
            exponent = jnp.where(position < lens[s], jnp.exp(scores), 0.0)
            den[s] = jnp.broadcast_to(
                jnp.sum(exponent, axis=-1, keepdims=True), den.shape[1:]
            )
            es[s] = exponent.astype(BF16)

    def attend(g):
        mine = slice(g * half, (g + 1) * half)
        for s in range(g * half, (g + 1) * half):
            if s % chunk == 0:
                vals[s // chunk].wait()
                if s // chunk + 2 < KEY_CHUNKS:
                    vals[s // chunk + 2].start()
            att[s] = mm(es[s], cv[s])
        here = own_exp[mine]
        att[mine] = (att[mine] + here * vf[mine]) / (den[mine] + here)
        if g == 0:
            proj[3].wait()
        heads = [
            (
                norm_scale(
                    att[mine, 2 * h, :] - lam[h] * att[mine, 2 * h + 1, :], head_gain
                )
                * HEAD_SCALE
            ).astype(BF16)
            for h in range(groups)
        ]
        part[g] = mm(jnp.concatenate(heads, axis=1), wo[...]).astype(BF16)

    swap = to_peer(part.at[other], part_in, 1, (me, other))

    def finish(g):
        swap.wait_recv()
        middle = residual[g * half : (g + 1) * half] + (
            part[g].astype(F32) + part_in[...].astype(F32)
        )
        middle = middle.astype(BF16).astype(F32)
        mid[...] = middle
        xs[me] = norm_scale(middle, row_of(cgain)).astype(BF16)
        each_peer(lambda peer: to_peer(xs.at[me], xs.at[me], 2, (peer, tp)).start())

    score(0)
    attend(0)

    @pl.when(tp == 1)
    def _():
        swap.start()

    score(1)

    @pl.when(tp == 0)
    def _():
        finish(0)

    attend(1)

    @pl.when(tp == 0)
    def _():
        swap.start()

    for i in (2, 3, 4, 5):
        own[i].start()
        swaps[i].start()

    @pl.when(tp == 1)
    def _():
        finish(1)

    swap.wait_send()
    for c in own:
        c.wait()
    for c in swaps:
        c.wait()
    all_but_one(tab, 0).wait()
    all_but_one(xs, 2).wait()

    count = n * half
    xf = xs[...].astype(F32).reshape(count, width)
    x = xf.astype(BF16)
    switch = 1.0 / (
        1.0 + jnp.exp(-jnp.sum(xf * row_of(mixer), axis=-1, keepdims=True))
    )
    table_all = tab[...].reshape(count, lanes)
    weight = jnp.sum(
        jnp.where(lax.broadcasted_iota(jnp.int32, (count, lanes), 1) == me, table_all, 0.0),
        axis=-1,
        keepdims=True,
    )
    total = None
    for gate, up, down, scale in ((eg, eu, ed, weight), (dg, du, dd, switch)):
        units = gate.shape[2]
        merge = units % 128 == 0
        for slots in ((0, 1),) if merge else ((0,), (1,)):
            gw = jnp.concatenate([gate[i] for i in slots], axis=1) if merge else gate[slots[0]]
            uw = jnp.concatenate([up[i] for i in slots], axis=1) if merge else up[slots[0]]
            dw = jnp.concatenate([down[i] for i in slots], axis=0) if merge else down[slots[0]]
            hidden = (silu(mm(x, gw)) * mm(x, uw) * scale).astype(BF16)
            term = mm(hidden, dw)
            total = term if total is None else total + term
    ys[...] = total.reshape(n, half, width).astype(BF16)
    rs[me] = ys[me]
    each_peer(lambda peer: to_peer(ys.at[peer], rs.at[me], 3, (peer, tp)).start())
    all_but_one(ys, 3).wait()
    ob[tp] = (mid[...] + jnp.sum(rs[...].astype(F32), axis=0)).astype(BF16)
    last = to_peer(ob.at[tp], ob.at[tp], 4, (me, other))
    last.start()
    last.wait()
    out_ref[...] = ob[...].astype(F32).reshape(seqs, width).astype(BF16)


def hand_over(*refs):
    count = (len(refs) - 1) // 2
    sem = refs[-1]
    copies = [
        pltpu.make_async_copy(source, target, sem.at[i])
        for i, (source, target) in enumerate(zip(refs[:count], refs[count : 2 * count]))
    ]
    for c in copies:
        c.start()
    for c in copies:
        c.wait()


def per_device(
    n,
    residual_in,
    lengths,
    cache_keys,
    cache_values,
    attend_gain,
    query_proj,
    key_proj,
    value_proj,
    lambdas,
    head_gain,
    out_proj,
    channel_gain,
    routes,
    route_weight,
    expert_gate,
    expert_up,
    expert_down,
    dense_gate,
    dense_up,
    dense_down,
    dense_mixer,
):
    seqs, width = residual_in.shape
    _, kv_local, length, key_width = cache_keys.shape
    value_width = cache_values.shape[3]
    half = seqs // 2
    lanes = -(-n // 128) * 128
    rows = 8
    inverse = ROTARY_BASE ** (-np.arange(HEAD // 2, dtype=np.float32) / (HEAD // 2))
    inverse = jnp.asarray(np.tile(inverse.astype(np.float32), 4)[None, :])
    vmem = pl.BlockSpec(memory_space=pltpu.VMEM)
    hbm = pl.BlockSpec(memory_space=pltpu.HBM)

    def two(w):
        return pltpu.VMEM((2,) + w.shape, BF16)

    eg, eu, ed = expert_gate[0], expert_up[0], expert_down[0]
    small = (
        lengths,
        lambdas,
        inverse,
        residual_in,
        attend_gain,
        head_gain,
        channel_gain,
        dense_mixer,
        routes.T,
        route_weight.T,
    )
    big = (
        cache_keys.reshape(seqs, length, key_width),
        cache_values.reshape(seqs, length, value_width),
        query_proj,
        key_proj,
        value_proj,
        out_proj,
        eg,
        eu,
        ed,
        dense_gate,
        dense_up,
        dense_down,
    )
    dma = pltpu.SemaphoreType.DMA
    results = ((seqs, width), (seqs, key_width), (seqs, value_width))
    out, nk, nv = pl.pallas_call(
        functools.partial(kernel, n),
        out_shape=tuple(pltpu.VMEM(shape, BF16) for shape in results),
        in_specs=[hbm] * (len(small) + len(big)),
        out_specs=(vmem, vmem, vmem),
        scratch_shapes=[pltpu.SMEM(a.shape, a.dtype) for a in small[:2]]
        + [pltpu.VMEM(a.shape, a.dtype) for a in small[2:]]
        + [pltpu.VMEM(w.shape, BF16) for w in big[:6]]
        + [two(w) for w in big[6:]]
        + [
            pltpu.VMEM((seqs, 2 * HEAD), F32),
            pltpu.VMEM((seqs, rows, key_width), F32),
            pltpu.VMEM((seqs, rows, length), BF16),
            pltpu.VMEM((seqs, rows, value_width), F32),
            pltpu.VMEM((seqs, rows, value_width), F32),
            pltpu.VMEM((2, half, width), BF16),
            pltpu.VMEM((half, width), BF16),
            pltpu.VMEM((half, width), F32),
            pltpu.VMEM((seqs, lanes), F32),
            pltpu.VMEM((n, half, lanes), F32),
            pltpu.VMEM((n, half, width), BF16),
            pltpu.VMEM((n, half, width), BF16),
            pltpu.VMEM((n, half, width), BF16),
            pltpu.VMEM((2, half, width), BF16),
            dma((len(small),)),
            dma((4,)),
            dma((KEY_CHUNKS,)),
            dma((KEY_CHUNKS,)),
            dma((6,)),
            dma((6,)),
            dma((6,)),
            dma((10,)),
        ],
        compiler_params=pltpu.CompilerParams(
            collective_id=0, has_side_effects=True, vmem_limit_bytes=56 * 1024 * 1024
        ),
    )(*(pltpu.with_memory_space_constraint(a, pltpu.HBM) for a in small + big))
    out, nk, nv = pl.pallas_call(
        hand_over,
        out_shape=tuple(jax.ShapeDtypeStruct(shape, BF16) for shape in results),
        in_specs=[vmem] * 3,
        out_specs=(hbm, hbm, hbm),
        scratch_shapes=[dma((3,))],
        compiler_params=pltpu.CompilerParams(vmem_limit_bytes=1024 * 1024),
    )(out, nk, nv)
    return (
        out,
        nk.reshape(seqs, kv_local, key_width),
        nv.reshape(seqs, kv_local, value_width),
    )


def solution(mesh):
    return jax.shard_map(
        functools.partial(per_device, mesh.shape["ep"]),
        mesh=mesh,
        in_specs=(
            P("ep", None),
            P("ep"),
            P("ep", "tp", None, None),
            P("ep", "tp", None, None),
            P(),
            P(None, "tp"),
            P(None, "tp"),
            P(None, "tp"),
            P("tp"),
            P(),
            P("tp", None),
            P(),
            P("ep", None),
            P("ep", None),
            P("ep", None, "tp"),
            P("ep", None, "tp"),
            P("ep", "tp", None),
            P(None, ("ep", "tp")),
            P(None, ("ep", "tp")),
            P(("ep", "tp"), None),
            P(),
        ),
        out_specs=(P("ep", None), P("ep", "tp", None), P("ep", "tp", None)),
        check_vma=False,
    )
```

time: 31.9 us -> 27.7 us (0.87)
  Pallas kernels: 31 us -> 26.8 us
    pallas_call x2, Pallas kernels: 31 us -> 26.8 us  [the longest x1 26.2 us: per_device(): pl.pallas_call(functools.partial(kernel, n), out_shape=tuple((pltpu.VMEM(...]
where the time goes in v1:
time: 27.7 us; the launch traced here: 27.5 us
  Pallas kernels  26.8 us (97%)
  between operations  0.65 us (2%)
    pallas_call x1, Pallas kernels, per_device(): pl.pallas_call(functools.partial(kernel, n), out_shape=tuple((pltpu.VMEM(...  26.2 us
    pallas_call x1, Pallas kernels, per_device(): pl.pallas_call(hand_over, out_shape=tuple((jax.ShapeDtypeStruct(shape, BF...  0.65 us

profile of v1, /device:TPU:0, one launch (start us, length us, event | category | flops | bytes accessed | tf_op | source)
XLA Modules:
  0.0 27.5 jit_solution(13002733275996846852)
XLA Ops:
  0.6 26.2 %shard_map.229 = (bf16[16,1024]{1,0:T(8,128)(2,1)S(1)}, bf16[16,128]{1,0:T(8,128)(2,1)S(1)}, bf16[16,128]{1,0:T(8,128)(2,1)S(1)}) custom-call(s32[16]{0:T(128)} %len_hbm.1, f32[2]{0:T(128)} %lam_hbm.1, f32[1,128]{1,0:T(1,128)} %constant.2.clone.inv_hbm, bf16[16,1024]{1,0:T(8,128)(2,1)} %res_hbm.1, bf16[1024]{0:T(1024)(128)(2,1)} %again_hbm.1, ...), custom_call_target="tpu_custom_call" | custom-call | tf_op jit(solution)/shard_map/pallas_call | solution.py:483
  26.8 0.6 %shard_map.230 = (bf16[16,1024]{1,0:T(8,128)(2,1)}, bf16[16,128]{1,0:T(8,128)(2,1)}, bf16[16,128]{1,0:T(8,128)(2,1)}) custom-call(bf16[16,1024]{1,0:T(8,128)(2,1)S(1)} %get-tuple-element.9.refs_0_, bf16[16,128]{1,0:T(8,128)(2,1)S(1)} %get-tuple-element.10.refs_1_, bf16[16,128]{1,0:T(8,128)(2,1)S(1)} %get-tuple-element.11.refs_2_), custom_call_target="tpu_custom_call" | custom-call | tf_op jit(solution)/shard_map/pallas_call | solution.py:520

commit v2 on v1

--- a/solution.py
+++ b/solution.py
@@ -13,6 +13,7 @@
 ROTARY_BASE = 10000.0
 HEAD_SCALE = 0.8
 KEY_CHUNKS = 4
+PASSES = 4
 MESH = pl.DeviceIdType.MESH
 F32 = jnp.float32
 BF16 = jnp.bfloat16
@@ -85,6 +86,9 @@
     du,
     dd,
     pos,
+    resf,
+    knew,
+    vnew,
     qs,
     es,
     den,
@@ -105,7 +109,8 @@
     own_sem,
     wsend,
     wrecv,
-    link,
+    sent,
+    got,
 ):
     seqs, width = res.shape
     half = xs.shape[1]
@@ -113,6 +118,15 @@
     tp = lax.axis_index("tp")
     other = 1 - tp
     chunk = seqs // KEY_CHUNKS
+    reach = n // PASSES
+    my_part = lax.div(me, reach)
+
+    def part_of(i):
+        group = other if i < KEY_CHUNKS // 2 else tp
+        return pl.ds(group * half + i % (KEY_CHUNKS // 2) * chunk, chunk)
+
+    def rows_of(group):
+        return pl.ds(pl.multiple_of(group * half, half), half)
 
     small = [
         pltpu.make_async_copy(a, b, small_sem.at[i])
@@ -136,15 +150,11 @@
         for i, (a, b) in enumerate(((wq_hbm, wq), (wk_hbm, wk), (wv_hbm, wv), (wo_hbm, wo)))
     ]
     keys = [
-        pltpu.make_async_copy(
-            ck_hbm.at[pl.ds(i * chunk, chunk)], ck.at[pl.ds(i * chunk, chunk)], key_sem.at[i]
-        )
+        pltpu.make_async_copy(ck_hbm.at[part_of(i)], ck.at[part_of(i)], key_sem.at[i])
         for i in range(KEY_CHUNKS)
     ]
     vals = [
-        pltpu.make_async_copy(
-            cv_hbm.at[pl.ds(i * chunk, chunk)], cv.at[pl.ds(i * chunk, chunk)], val_sem.at[i]
-        )
+        pltpu.make_async_copy(cv_hbm.at[part_of(i)], cv.at[part_of(i)], val_sem.at[i])
         for i in range(KEY_CHUNKS)
     ]
     weight_pairs = (
@@ -158,7 +168,7 @@
     own = [
         pltpu.make_async_copy(a, b.at[0], own_sem.at[i]) for i, (a, b) in enumerate(weight_pairs)
     ]
-    for c in small[:4] + proj[:3] + keys[:1] + small[4:] + keys[1:2]:
+    for c in small[:4] + proj[:3] + small[4:]:
         c.start()
 
     bar = pltpu.get_barrier_semaphore()
@@ -171,6 +181,7 @@
         return c
 
     lax.fori_loop(1, n, greet, 0)
+    keys[0].start()
 
     small[0].wait()
     for s in range(seqs):
@@ -192,17 +203,32 @@
 
     small[2].wait()
     small[3].wait()
-    residual = res[...].astype(F32)
-    normed = norm_scale(residual, row_of(again)).astype(BF16)
+    for c in keys[1:2] + vals[:2]:
+        c.start()
+    resf[...] = res[...].astype(F32)
+    normed = norm_scale(resf[...], row_of(again)).astype(BF16)
+    for c in small[4:]:
+        c.wait()
+    expert_row = lax.broadcasted_iota(jnp.int32, (n, 1, seqs), 0)
+    routes = routes_v[...].reshape(-1, 1, 1, seqs)
+    rweights = rw_v[...].reshape(-1, 1, 1, seqs)
+    table = jnp.zeros((n, 1, seqs), F32)
+    for k in range(routes.shape[0]):
+        table = table + jnp.where(expert_row == routes[k], rweights[k], 0.0)
+    tabf[...] = jnp.zeros_like(tabf)
+    tabf[:, :, 0:seqs] = table
+    tab[me] = tabf[me]
     for c in proj[:3]:
         c.wait()
-    for c in vals[:2] + proj[3:]:
+    for c in keys[2:] + proj[3:]:
         c.start()
     queries = mm(normed, wq[...])
     new_keys = rotate(mm(normed, wk[...]))
     new_values = mm(normed, wv[...]).astype(BF16)
     nk_ref[...] = new_keys
     nv_ref[...] = new_values
+    knew[...] = new_keys.astype(F32)
+    vnew[...] = new_values.astype(F32)
     groups = queries.shape[1] // (2 * HEAD)
     rows = qs.shape[1]
     qs[...] = jnp.zeros_like(qs)
@@ -213,35 +239,25 @@
         for m in range(2):
             qs[:, 2 * g + m, :] = jnp.where(lane // HEAD == m, turned, 0.0)
 
-    for c in small[4:]:
-        c.wait()
-    lanes = tabf.shape[1]
-    expert_row = lax.broadcasted_iota(jnp.int32, (lanes, seqs), 0)
-    routes = routes_v[...]
-    rweights = rw_v[...]
-    table = jnp.zeros((lanes, seqs), F32)
-    for k in range(routes.shape[0]):
-        table = table + jnp.where(expert_row == routes[k : k + 1], rweights[k : k + 1], 0.0)
-    tabf[...] = table.T
-    mine = pl.ds(pl.multiple_of(tp * half, half), half)
-    tab[me] = tabf[mine, :]
-
-    def to_peer(src, dst, k, peer):
+    def to_peer(src, dst, k, peer, r=None):
         return pltpu.make_async_remote_copy(
             src_ref=src,
             dst_ref=dst,
-            send_sem=link.at[2 * k],
-            recv_sem=link.at[2 * k + 1],
+            send_sem=sent.at[k],
+            recv_sem=got.at[k if r is None else r],
             device_id=peer,
             device_id_type=MESH,
         )
 
-    def each_peer(send):
-        if n & (n - 1) == 0 and n <= 16:
-            bits = [lax.rem(lax.div(me, 1 << b), 2) for b in range(n.bit_length() - 1)]
-            for k in range(n - 1, 0, -1):
+    low = lax.rem(me, reach)
+
+    def each_peer(send, h):
+        if reach & (reach - 1) == 0 and reach <= 8:
+            bits = [lax.rem(lax.div(low, 1 << b), 2) for b in range(reach.bit_length() - 1)]
+            for k in range(reach - 1, 0, -1):
                 send(
-                    sum(
+                    h * reach
+                    + sum(
                         (1 << b) * (1 - bit if k >> b & 1 else bit)
                         for b, bit in enumerate(bits)
                     )
@@ -249,16 +265,19 @@
         else:
 
             def step(k, c):
-                send(lax.rem(me + k, n))
+                send(h * reach + lax.rem(low + k, reach))
                 return c
 
-            lax.fori_loop(1, n, step, 0)
-
-    def all_but_one(buffer, k):
-        block = buffer.at[pl.ds(0, n - 1)]
-        return to_peer(block, block, k, (me, other))
-
-    pl.semaphore_wait(bar, n)
+            lax.fori_loop(1, reach, step, 0)
+
+        @pl.when(my_part != h)
+        def _():
+            send(h * reach + low)
+
+    def blocks(buffer, count, k, r=None):
+        block = buffer.at[pl.ds(0, count)]
+        return to_peer(block, block, k, (me, other), r)
+
     swaps = [
         pltpu.make_async_remote_copy(
             src_ref=a,
@@ -270,23 +289,14 @@
         )
         for i, (a, b) in enumerate(weight_pairs)
     ]
-    for i in (0, 1):
-        own[i].start()
-        swaps[i].start()
-    each_peer(lambda peer: to_peer(tab.at[me], tab.at[me], 0, (peer, tp)).start())
-
     position = lax.broadcasted_iota(jnp.int32, (rows, ck.shape[1]), 1)
-    kf = new_keys.astype(F32).reshape(seqs, 1, 2 * HEAD)
-    vf = new_values.astype(F32).reshape(seqs, 1, new_values.shape[1])
-    own_exp = jnp.exp(jnp.sum(qs[...] * kf, axis=-1, keepdims=True))
     head_gain = row_of(hgain)
 
-    def score(g):
-        for s in range(g * half, (g + 1) * half):
-            if s % chunk == 0:
-                keys[s // chunk].wait()
-                if s // chunk + 2 < KEY_CHUNKS:
-                    keys[s // chunk + 2].start()
+    def score(group, first):
+        for i in range(half):
+            if i % chunk == 0:
+                keys[(0 if first else KEY_CHUNKS // 2) + i // chunk].wait()
+            s = group * half + i
             scores = lax.dot_general(
                 qs[s].astype(BF16), ck[s], (((1,), (1,)), ((), ())), preferred_element_type=F32
             )
@@ -296,105 +306,103 @@
             )
             es[s] = exponent.astype(BF16)
 
-    def attend(g):
-        mine = slice(g * half, (g + 1) * half)
-        for s in range(g * half, (g + 1) * half):
-            if s % chunk == 0:
-                vals[s // chunk].wait()
-                if s // chunk + 2 < KEY_CHUNKS:
-                    vals[s // chunk + 2].start()
+    def attend(group, first):
+        for i in range(half):
+            if i % chunk == 0:
+                vals[(0 if first else KEY_CHUNKS // 2) + i // chunk].wait()
+            s = group * half + i
             att[s] = mm(es[s], cv[s])
-        here = own_exp[mine]
-        att[mine] = (att[mine] + here * vf[mine]) / (den[mine] + here)
-        if g == 0:
+        here = rows_of(group)
+        kf = knew[here, :].reshape(half, 1, 2 * HEAD)
+        vf = vnew[here, :].reshape(half, 1, vnew.shape[1])
+        own_exp = jnp.exp(jnp.sum(qs[here] * kf, axis=-1, keepdims=True))
+        att[here] = (att[here] + own_exp * vf) / (den[here] + own_exp)
+        if first:
             proj[3].wait()
         heads = [
             (
                 norm_scale(
-                    att[mine, 2 * h, :] - lam[h] * att[mine, 2 * h + 1, :], head_gain
+                    att[here, 2 * h, :] - lam[h] * att[here, 2 * h + 1, :], head_gain
                 )
                 * HEAD_SCALE
             ).astype(BF16)
             for h in range(groups)
         ]
-        part[g] = mm(jnp.concatenate(heads, axis=1), wo[...]).astype(BF16)
-
-    swap = to_peer(part.at[other], part_in, 1, (me, other))
-
-    def finish(g):
-        swap.wait_recv()
-        middle = residual[g * half : (g + 1) * half] + (
-            part[g].astype(F32) + part_in[...].astype(F32)
-        )
-        middle = middle.astype(BF16).astype(F32)
-        mid[...] = middle
-        xs[me] = norm_scale(middle, row_of(cgain)).astype(BF16)
-        each_peer(lambda peer: to_peer(xs.at[me], xs.at[me], 2, (peer, tp)).start())
-
-    score(0)
-    attend(0)
-
-    @pl.when(tp == 1)
-    def _():
-        swap.start()
-
-    score(1)
-
-    @pl.when(tp == 0)
-    def _():
-        finish(0)
-
-    attend(1)
-
-    @pl.when(tp == 0)
-    def _():
-        swap.start()
-
-    for i in (2, 3, 4, 5):
-        own[i].start()
+        return mm(jnp.concatenate(heads, axis=1), wo[...]).astype(BF16)
+
+    score(other, True)
+    for c in vals[2:]:
+        c.start()
+    part[...] = attend(other, True)
+    for c in own:
+        c.start()
+    score(tp, False)
+    pl.semaphore_wait(bar, n)
+    swap = to_peer(part, part_in, 1, (me, other))
+    swap.start()
+    for h in range(PASSES):
+        each_peer(lambda peer: to_peer(tabf.at[peer], tab.at[me], 0, (peer, tp)).start(), h)
+    for i in (0, 1, 3, 4, 2, 5):
         swaps[i].start()
-
-    @pl.when(tp == 1)
-    def _():
-        finish(1)
-
-    swap.wait_send()
+    partial = attend(tp, False)
+    swap.wait()
+    middle = resf[rows_of(tp), :] + (partial.astype(F32) + part_in[...].astype(F32))
+    middle = middle.astype(BF16).astype(F32)
+    mid[...] = middle
+    xs[me] = norm_scale(middle, row_of(cgain)).astype(BF16)
+    for k in range(PASSES):
+        h = 2 * lax.rem(lax.div(my_part, 2) + k // 2, 2) + lax.rem(lax.rem(my_part, 2) + k % 2, 2)
+        each_peer(
+            lambda peer: to_peer(xs.at[me], xs.at[me], 2, (peer, tp), 4 + my_part).start(), h
+        )
     for c in own:
         c.wait()
     for c in swaps:
         c.wait()
-    all_but_one(tab, 0).wait()
-    all_but_one(xs, 2).wait()
-
-    count = n * half
-    xf = xs[...].astype(F32).reshape(count, width)
-    x = xf.astype(BF16)
-    switch = 1.0 / (
-        1.0 + jnp.exp(-jnp.sum(xf * row_of(mixer), axis=-1, keepdims=True))
-    )
-    table_all = tab[...].reshape(count, lanes)
-    weight = jnp.sum(
-        jnp.where(lax.broadcasted_iota(jnp.int32, (count, lanes), 1) == me, table_all, 0.0),
-        axis=-1,
-        keepdims=True,
-    )
-    total = None
-    for gate, up, down, scale in ((eg, eu, ed, weight), (dg, du, dd, switch)):
-        units = gate.shape[2]
-        merge = units % 128 == 0
-        for slots in ((0, 1),) if merge else ((0,), (1,)):
-            gw = jnp.concatenate([gate[i] for i in slots], axis=1) if merge else gate[slots[0]]
-            uw = jnp.concatenate([up[i] for i in slots], axis=1) if merge else up[slots[0]]
-            dw = jnp.concatenate([down[i] for i in slots], axis=0) if merge else down[slots[0]]
-            hidden = (silu(mm(x, gw)) * mm(x, uw) * scale).astype(BF16)
-            term = mm(hidden, dw)
-            total = term if total is None else total + term
-    ys[...] = total.reshape(n, half, width).astype(BF16)
+    blocks(tab, n - 1, 0).wait()
+
+    count = reach * half
+
+    def pass_over(h):
+        for inside in (0, 1):
+
+            @pl.when(my_part == h if inside else my_part != h)
+            def _():
+                blocks(xs, reach - inside, 2, 4 + h).wait_recv()
+
+        here = slice(h * reach, (h + 1) * reach)
+        xf = xs[here].astype(F32).reshape(count, width)
+        x = xf.astype(BF16)
+        switch = 1.0 / (
+            1.0 + jnp.exp(-jnp.sum(xf * row_of(mixer), axis=-1, keepdims=True))
+        )
+        shape = (reach, half, tab.shape[2])
+        token = lax.broadcasted_iota(jnp.int32, shape, 1) + tp * half
+        spot = lax.broadcasted_iota(jnp.int32, shape, 2)
+        weight = jnp.sum(
+            jnp.where(spot == token, tab[here], 0.0), axis=-1, keepdims=True
+        ).reshape(count, 1)
+        total = None
+        for gate, up, down, scale in ((eg, eu, ed, weight), (dg, du, dd, switch)):
+            units = gate.shape[2]
+            merge = units % 128 == 0
+            for slots in ((0, 1),) if merge else ((0,), (1,)):
+                gw = jnp.concatenate([gate[i] for i in slots], axis=1) if merge else gate[slots[0]]
+                uw = jnp.concatenate([up[i] for i in slots], axis=1) if merge else up[slots[0]]
+                dw = jnp.concatenate([down[i] for i in slots], axis=0) if merge else down[slots[0]]
+                hidden = (silu(mm(x, gw)) * mm(x, uw) * scale).astype(BF16)
+                term = mm(hidden, dw)
+                total = term if total is None else total + term
+        ys[here] = total.reshape(reach, half, width).astype(BF16)
+        each_peer(lambda peer: to_peer(ys.at[peer], rs.at[me], 3, (peer, tp)).start(), h)
+
+    for h in range(PASSES):
+        pass_over(h)
     rs[me] = ys[me]
-    each_peer(lambda peer: to_peer(ys.at[peer], rs.at[me], 3, (peer, tp)).start())
-    all_but_one(ys, 3).wait()
+    blocks(xs, n - 1, 2).wait_send()
+    blocks(ys, n - 1, 3).wait()
     ob[tp] = (mid[...] + jnp.sum(rs[...].astype(F32), axis=0)).astype(BF16)
-    last = to_peer(ob.at[tp], ob.at[tp], 4, (me, other))
+    last = to_peer(ob.at[tp], ob.at[tp], 4, (me, other), 2)
     last.start()
     last.wait()
     out_ref[...] = ob[...].astype(F32).reshape(seqs, width).astype(BF16)
@@ -441,7 +449,7 @@
     _, kv_local, length, key_width = cache_keys.shape
     value_width = cache_values.shape[3]
     half = seqs // 2
-    lanes = -(-n // 128) * 128
+    lanes = -(-seqs // 128) * 128
     rows = 8
     inverse = ROTARY_BASE ** (-np.arange(HEAD // 2, dtype=np.float32) / (HEAD // 2))
     inverse = jnp.asarray(np.tile(inverse.astype(np.float32), 4)[None, :])
@@ -491,15 +499,18 @@
         + [two(w) for w in big[6:]]
         + [
             pltpu.VMEM((seqs, 2 * HEAD), F32),
+            pltpu.VMEM((seqs, width), F32),
+            pltpu.VMEM((seqs, key_width), F32),
+            pltpu.VMEM((seqs, value_width), F32),
             pltpu.VMEM((seqs, rows, key_width), F32),
             pltpu.VMEM((seqs, rows, length), BF16),
             pltpu.VMEM((seqs, rows, value_width), F32),
             pltpu.VMEM((seqs, rows, value_width), F32),
-            pltpu.VMEM((2, half, width), BF16),
+            pltpu.VMEM((half, width), BF16),
             pltpu.VMEM((half, width), BF16),
             pltpu.VMEM((half, width), F32),
-            pltpu.VMEM((seqs, lanes), F32),
-            pltpu.VMEM((n, half, lanes), F32),
+            pltpu.VMEM((n, 1, lanes), F32),
+            pltpu.VMEM((n, 1, lanes), F32),
             pltpu.VMEM((n, half, width), BF16),
             pltpu.VMEM((n, half, width), BF16),
             pltpu.VMEM((n, half, width), BF16),
@@ -511,7 +522,8 @@
             dma((6,)),
             dma((6,)),
             dma((6,)),
-            dma((10,)),
+            dma((5,)),
+            dma((4 + PASSES,)),
         ],
         compiler_params=pltpu.CompilerParams(
             collective_id=0, has_side_effects=True, vmem_limit_bytes=56 * 1024 * 1024

time: 27.7 us -> 24.4 us (0.88)
  Pallas kernels: 26.8 us -> 23.6 us
    pallas_call x1, Pallas kernels: 26.2 us -> 23 us  [per_device(): pl.pallas_call(functools.partial(kernel, n), out_shape=tuple((pltpu.VMEM(...]
where the time goes in v2:
time: 24.4 us; the launch traced here: 24.3 us
  Pallas kernels  23.6 us (97%)
  between operations  0.65 us (3%)
    pallas_call x1, Pallas kernels, per_device(): pl.pallas_call(functools.partial(kernel, n), out_shape=tuple((pltpu.VMEM(...  23 us
    pallas_call x1, Pallas kernels, per_device(): pl.pallas_call(hand_over, out_shape=tuple((jax.ShapeDtypeStruct(shape, BF...  0.65 us

profile of v2, /device:TPU:0, one launch (start us, length us, event | category | flops | bytes accessed | tf_op | source)
XLA Modules:
  0.0 24.3 jit_solution(692193637907458409)
XLA Ops:
  0.6 23.0 %shard_map.229 = (bf16[16,1024]{1,0:T(8,128)(2,1)S(1)}, bf16[16,128]{1,0:T(8,128)(2,1)S(1)}, bf16[16,128]{1,0:T(8,128)(2,1)S(1)}) custom-call(s32[16]{0:T(128)} %len_hbm.1, f32[2]{0:T(128)} %lam_hbm.1, f32[1,128]{1,0:T(1,128)} %constant.2.clone.inv_hbm, bf16[16,1024]{1,0:T(8,128)(2,1)} %res_hbm.1, bf16[1024]{0:T(1024)(128)(2,1)} %again_hbm.1, ...), custom_call_target="tpu_custom_call" | custom-call | tf_op jit(solution)/shard_map/pallas_call | solution.py:491
  23.6 0.6 %shard_map.230 = (bf16[16,1024]{1,0:T(8,128)(2,1)}, bf16[16,128]{1,0:T(8,128)(2,1)}, bf16[16,128]{1,0:T(8,128)(2,1)}) custom-call(bf16[16,1024]{1,0:T(8,128)(2,1)S(1)} %get-tuple-element.9.refs_0_, bf16[16,128]{1,0:T(8,128)(2,1)S(1)} %get-tuple-element.10.refs_1_, bf16[16,128]{1,0:T(8,128)(2,1)S(1)} %get-tuple-element.11.refs_2_), custom_call_target="tpu_custom_call" | custom-call | tf_op jit(solution)/shard_map/pallas_call | solution.py:532

commit v3 on v2

--- a/solution.py
+++ b/solution.py
@@ -14,6 +14,8 @@
 HEAD_SCALE = 0.8
 KEY_CHUNKS = 4
 PASSES = 4
+SEND_ORDER = ((0, 1, 2, 3), (1, 0, 3, 2), (2, 1, 0, 3), (3, 2, 1, 0))
+GROUPS = ((0, 1), (1, 1), (2, 2))
 MESH = pl.DeviceIdType.MESH
 F32 = jnp.float32
 BF16 = jnp.bfloat16
@@ -121,6 +123,13 @@
     reach = n // PASSES
     my_part = lax.div(me, reach)
 
+    high, odd = lax.div(my_part, 2), lax.rem(my_part, 2)
+
+    def in_order(table):
+        near = [a + odd * (b - a) for a, b in zip(table[0], table[1])]
+        far = [a + odd * (b - a) for a, b in zip(table[2], table[3])]
+        return [a + high * (b - a) for a, b in zip(near, far)]
+
     def part_of(i):
         group = other if i < KEY_CHUNKS // 2 else tp
         return pl.ds(group * half + i % (KEY_CHUNKS // 2) * chunk, chunk)
@@ -165,12 +174,15 @@
         (du_hbm, du),
         (dd_hbm, dd),
     )
+    whole = own_sem.shape[0] == 1
     own = [
-        pltpu.make_async_copy(a, b.at[0], own_sem.at[i]) for i, (a, b) in enumerate(weight_pairs)
+        pltpu.make_async_copy(a, b.at[0], own_sem.at[0 if whole else i])
+        for i, (a, b) in enumerate(weight_pairs)
     ]
     for c in small[:4] + proj[:3] + small[4:]:
         c.start()
 
+    keys[0].start()
     bar = pltpu.get_barrier_semaphore()
     pl.semaphore_signal(bar, inc=1, device_id=(me, other), device_id_type=MESH)
 
@@ -181,8 +193,8 @@
         return c
 
     lax.fori_loop(1, n, greet, 0)
-    keys[0].start()
-
+
+    keys[1].start()
     small[0].wait()
     for s in range(seqs):
         pos[s : s + 1, :] = jnp.full((1, 2 * HEAD), lens[s].astype(F32), F32)
@@ -203,7 +215,7 @@
 
     small[2].wait()
     small[3].wait()
-    for c in keys[1:2] + vals[:2]:
+    for c in vals[:2]:
         c.start()
     resf[...] = res[...].astype(F32)
     normed = norm_scale(resf[...], row_of(again)).astype(BF16)
@@ -282,8 +294,8 @@
         pltpu.make_async_remote_copy(
             src_ref=a,
             dst_ref=b.at[1],
-            send_sem=wsend.at[i],
-            recv_sem=wrecv.at[i],
+            send_sem=wsend.at[0 if whole else i],
+            recv_sem=wrecv.at[0 if whole else i],
             device_id=(me, other),
             device_id_type=MESH,
         )
@@ -336,47 +348,68 @@
     part[...] = attend(other, True)
     for c in own:
         c.start()
+    swap = to_peer(part, part_in, 1, (me, other))
+
+    def open_links():
+        pl.semaphore_wait(bar, n)
+        swap.start()
+        for h in range(PASSES):
+            each_peer(
+                lambda peer: to_peer(
+                    tabf.at[peer], tab.at[me], 0, (peer, tp), 4 + PASSES + my_part
+                ).start(),
+                h,
+            )
+        for i in (0, 1, 3, 4, 2, 5):
+            swaps[i].start()
+
+    pl.when(high == 1)(open_links)
     score(tp, False)
-    pl.semaphore_wait(bar, n)
-    swap = to_peer(part, part_in, 1, (me, other))
-    swap.start()
-    for h in range(PASSES):
-        each_peer(lambda peer: to_peer(tabf.at[peer], tab.at[me], 0, (peer, tp)).start(), h)
-    for i in (0, 1, 3, 4, 2, 5):
-        swaps[i].start()
+    pl.when(high == 0)(open_links)
     partial = attend(tp, False)
     swap.wait()
     middle = resf[rows_of(tp), :] + (partial.astype(F32) + part_in[...].astype(F32))
     middle = middle.astype(BF16).astype(F32)
     mid[...] = middle
     xs[me] = norm_scale(middle, row_of(cgain)).astype(BF16)
-    for k in range(PASSES):
-        h = 2 * lax.rem(lax.div(my_part, 2) + k // 2, 2) + lax.rem(lax.rem(my_part, 2) + k % 2, 2)
+    for h in in_order(SEND_ORDER):
         each_peer(
             lambda peer: to_peer(xs.at[me], xs.at[me], 2, (peer, tp), 4 + my_part).start(), h
         )
-    for c in own:
-        c.wait()
-    for c in swaps:
-        c.wait()
-    blocks(tab, n - 1, 0).wait()
-
-    count = reach * half
-
-    def pass_over(h):
-        for inside in (0, 1):
-
-            @pl.when(my_part == h if inside else my_part != h)
-            def _():
-                blocks(xs, reach - inside, 2, 4 + h).wait_recv()
-
-        here = slice(h * reach, (h + 1) * reach)
+    if whole:
+        size = sum(a.shape[0] * a.shape[1] for a, _ in weight_pairs)
+        like = ck.at[pl.ds(0, size // (ck.shape[1] * ck.shape[2]))]
+        pltpu.make_async_copy(like, like, own_sem.at[0]).wait()
+        pltpu.make_async_remote_copy(
+            src_ref=like,
+            dst_ref=like,
+            send_sem=wsend.at[0],
+            recv_sem=wrecv.at[0],
+            device_id=(me, other),
+            device_id_type=MESH,
+        ).wait()
+    else:
+        for c in own + swaps:
+            c.wait()
+    blocks(tab, n - 1, 0).wait_send()
+
+    def pass_over(first, parts):
+        for h in range(first, first + parts):
+            for inside in (0, 1):
+
+                @pl.when(my_part == h if inside else my_part != h)
+                def _():
+                    blocks(tab, reach - inside, 0, 4 + PASSES + h).wait_recv()
+                    blocks(xs, reach - inside, 2, 4 + h).wait_recv()
+
+        here = slice(first * reach, (first + parts) * reach)
+        count = parts * reach * half
         xf = xs[here].astype(F32).reshape(count, width)
         x = xf.astype(BF16)
         switch = 1.0 / (
             1.0 + jnp.exp(-jnp.sum(xf * row_of(mixer), axis=-1, keepdims=True))
         )
-        shape = (reach, half, tab.shape[2])
+        shape = (parts * reach, half, tab.shape[2])
         token = lax.broadcasted_iota(jnp.int32, shape, 1) + tp * half
         spot = lax.broadcasted_iota(jnp.int32, shape, 2)
         weight = jnp.sum(
@@ -393,11 +426,12 @@
                 hidden = (silu(mm(x, gw)) * mm(x, uw) * scale).astype(BF16)
                 term = mm(hidden, dw)
                 total = term if total is None else total + term
-        ys[here] = total.reshape(reach, half, width).astype(BF16)
-        each_peer(lambda peer: to_peer(ys.at[peer], rs.at[me], 3, (peer, tp)).start(), h)
-
-    for h in range(PASSES):
-        pass_over(h)
+        ys[here] = total.reshape(parts * reach, half, width).astype(BF16)
+        for h in range(first, first + parts):
+            each_peer(lambda peer: to_peer(ys.at[peer], rs.at[me], 3, (peer, tp)).start(), h)
+
+    for first, parts in GROUPS:
+        pass_over(first, parts)
     rs[me] = ys[me]
     blocks(xs, n - 1, 2).wait_send()
     blocks(ys, n - 1, 3).wait()
@@ -487,6 +521,10 @@
         dense_down,
     )
     dma = pltpu.SemaphoreType.DMA
+    weights = big[6:]
+    size = sum(w.size for w in weights)
+    even = all(w.shape[1] % 128 == 0 for w in weights) and size % (length * key_width) == 0
+    waits = 1 if even and size <= seqs * length * key_width else len(weights)
     results = ((seqs, width), (seqs, key_width), (seqs, value_width))
     out, nk, nv = pl.pallas_call(
         functools.partial(kernel, n),
@@ -519,11 +557,11 @@
             dma((4,)),
             dma((KEY_CHUNKS,)),
             dma((KEY_CHUNKS,)),
-            dma((6,)),
-            dma((6,)),
-            dma((6,)),
+            dma((waits,)),
+            dma((waits,)),
+            dma((waits,)),
             dma((5,)),
-            dma((4 + PASSES,)),
+            dma((4 + 2 * PASSES,)),
         ],
         compiler_params=pltpu.CompilerParams(
             collective_id=0, has_side_effects=True, vmem_limit_bytes=56 * 1024 * 1024

time: 24.4 us -> 24.3 us (level)
  no operation moved by 1% of the time
where the time goes in v3:
time: 24.3 us; the launch traced here: 24.2 us
  Pallas kernels  23.5 us (97%)
  between operations  0.65 us (3%)
    pallas_call x1, Pallas kernels, per_device(): pl.pallas_call(functools.partial(kernel, n), out_shape=tuple((pltpu.VMEM(...  22.9 us
    pallas_call x1, Pallas kernels, per_device(): pl.pallas_call(hand_over, out_shape=tuple((jax.ShapeDtypeStruct(shape, BF...  0.65 us

profile of v3, /device:TPU:0, one launch (start us, length us, event | category | flops | bytes accessed | tf_op | source)
XLA Modules:
  0.0 24.2 jit_solution(7932068665522220322)
XLA Ops:
  0.6 22.9 %shard_map.229 = (bf16[16,1024]{1,0:T(8,128)(2,1)S(1)}, bf16[16,128]{1,0:T(8,128)(2,1)S(1)}, bf16[16,128]{1,0:T(8,128)(2,1)S(1)}) custom-call(s32[16]{0:T(128)} %len_hbm.1, f32[2]{0:T(128)} %lam_hbm.1, f32[1,128]{1,0:T(1,128)} %constant.2.clone.inv_hbm, bf16[16,1024]{1,0:T(8,128)(2,1)} %res_hbm.1, bf16[1024]{0:T(1024)(128)(2,1)} %again_hbm.1, ...), custom_call_target="tpu_custom_call" | custom-call | tf_op jit(solution)/shard_map/pallas_call | solution.py:529
  23.5 0.6 %shard_map.230 = (bf16[16,1024]{1,0:T(8,128)(2,1)}, bf16[16,128]{1,0:T(8,128)(2,1)}, bf16[16,128]{1,0:T(8,128)(2,1)}) custom-call(bf16[16,1024]{1,0:T(8,128)(2,1)S(1)} %get-tuple-element.9.refs_0_, bf16[16,128]{1,0:T(8,128)(2,1)S(1)} %get-tuple-element.10.refs_1_, bf16[16,128]{1,0:T(8,128)(2,1)S(1)} %get-tuple-element.11.refs_2_), custom_call_target="tpu_custom_call" | custom-call | tf_op jit(solution)/shard_map/pallas_call | solution.py:570

commit v4 on v3

--- a/solution.py
+++ b/solution.py
@@ -372,14 +372,23 @@
     middle = middle.astype(BF16).astype(F32)
     mid[...] = middle
     xs[me] = norm_scale(middle, row_of(cgain)).astype(BF16)
-    for h in in_order(SEND_ORDER):
+    def give_rows(h):
         each_peer(
             lambda peer: to_peer(xs.at[me], xs.at[me], 2, (peer, tp), 4 + my_part).start(), h
         )
+
+    order = in_order(SEND_ORDER)
+    for k, h in enumerate(order):
+        if k < 2:
+            give_rows(h)
+        else:
+            pl.when(tp == 0)(lambda: give_rows(h))
     if whole:
         size = sum(a.shape[0] * a.shape[1] for a, _ in weight_pairs)
         like = ck.at[pl.ds(0, size // (ck.shape[1] * ck.shape[2]))]
         pltpu.make_async_copy(like, like, own_sem.at[0]).wait()
+        for h in order[2:]:
+            pl.when(tp == 1)(lambda: give_rows(h))
         pltpu.make_async_remote_copy(
             src_ref=like,
             dst_ref=like,
@@ -389,6 +398,8 @@
             device_id_type=MESH,
         ).wait()
     else:
+        for h in order[2:]:
+            pl.when(tp == 1)(lambda: give_rows(h))
         for c in own + swaps:
             c.wait()
     blocks(tab, n - 1, 0).wait_send()

time: 24.3 us -> 24.3 us (level)
  no operation moved by 1% of the time
where the time goes in v4:
time: 24.3 us; the launch traced here: 24.2 us
  Pallas kernels  23.5 us (97%)
  between operations  0.65 us (3%)
    pallas_call x1, Pallas kernels, per_device(): pl.pallas_call(functools.partial(kernel, n), out_shape=tuple((pltpu.VMEM(...  22.9 us
    pallas_call x1, Pallas kernels, per_device(): pl.pallas_call(hand_over, out_shape=tuple((jax.ShapeDtypeStruct(shape, BF...  0.65 us

profile of v4, /device:TPU:0, one launch (start us, length us, event | category | flops | bytes accessed | tf_op | source)
XLA Modules:
  0.0 24.2 jit_solution(8088091816742921219)
XLA Ops:
  0.6 22.9 %shard_map.229 = (bf16[16,1024]{1,0:T(8,128)(2,1)S(1)}, bf16[16,128]{1,0:T(8,128)(2,1)S(1)}, bf16[16,128]{1,0:T(8,128)(2,1)S(1)}) custom-call(s32[16]{0:T(128)} %len_hbm.1, f32[2]{0:T(128)} %lam_hbm.1, f32[1,128]{1,0:T(1,128)} %constant.2.clone.inv_hbm, bf16[16,1024]{1,0:T(8,128)(2,1)} %res_hbm.1, bf16[1024]{0:T(1024)(128)(2,1)} %again_hbm.1, ...), custom_call_target="tpu_custom_call" | custom-call | tf_op jit(solution)/shard_map/pallas_call | solution.py:540
  23.5 0.6 %shard_map.230 = (bf16[16,1024]{1,0:T(8,128)(2,1)}, bf16[16,128]{1,0:T(8,128)(2,1)}, bf16[16,128]{1,0:T(8,128)(2,1)}) custom-call(bf16[16,1024]{1,0:T(8,128)(2,1)S(1)} %get-tuple-element.9.refs_0_, bf16[16,128]{1,0:T(8,128)(2,1)S(1)} %get-tuple-element.10.refs_1_, bf16[16,128]{1,0:T(8,128)(2,1)S(1)} %get-tuple-element.11.refs_2_), custom_call_target="tpu_custom_call" | custom-call | tf_op jit(solution)/shard_map/pallas_call | solution.py:581
